TPU v7x, 32 devices: a whole 2x2x4 slice. The times are simulated.
32 devices in a mesh: sp: 8 (over z, y), tp: 4 (over x, core).
Axes of the slice: x: 2, y: 2, z: 4, core: 2. Of those that a mesh axis runs over, the one named last changes fastest.
Arguments:
- queries_nope: bfloat16 [3072, 8, 128], P('sp', 'tp'), may hold values from -9 to 9
- queries_rope: bfloat16 [3072, 8, 64], P('sp', 'tp'), may hold values from -6 to 6
- latent: bfloat16 [3072, 512], P('sp'), may hold values from -8 to 8, as said below
- rope_key: bfloat16 [3072, 64], P('sp'), may hold values from -6 to 6
- latent_gain: float32 [512], replicated, may hold values from 0.1 to 1.9
- key_up: bfloat16 [512, 1024], P(None, 'tp'), may hold values from -0.25 to 0.25
- value_up: bfloat16 [512, 1024], P(None, 'tp'), may hold values from -0.25 to 0.25
- out_proj: bfloat16 [1024, 2048], P('tp'), may hold values from -0.75 to 0.75
- stream: bfloat16 [3072, 2048], P(('sp', 'tp')), may hold values from -6 to 6
- mix_gain: float32 [2048], replicated, may hold values from 0.1 to 1.9
- w_gate: bfloat16 [2048, 3072], P('sp', 'tp'), may hold values from -0.125 to 0.125
- w_up: bfloat16 [2048, 3072], P('sp', 'tp'), may hold values from -0.125 to 0.125
- w_down: bfloat16 [3072, 2048], P('tp', 'sp'), may hold values from -0.4375 to 0.4375
- mlp_gain: float32 [2048], replicated, may hold values from 0.1 to 1.9
Outputs:
- result: bfloat16 [3072, 2048], P(('sp', 'tp'))
Inputs may be any that keep to these rules, and one draw needn't show every extreme that they name: latent rows carry a mean vector that changes from one eighth of the sequence to the next.
All inputs are finite; a program needn't handle non-finite values.
Results may differ from a plain program's by a relative error of at most 0.017.
Values may be sent and summed in bfloat16 or wider, within the bound.
A program may use at most 192 MiB of HBM per device.

v0:
```python
import jax
import jax.numpy as jnp
from jax import lax
from jax.sharding import PartitionSpec as P

theta_base = 10000.0
residual_weight = 8.0**0.25
norm_floor = 1.0
big_negative = -1e30


def rotate(vector, first_row):
    half = vector.shape[-1] // 2
    rates = theta_base ** (-2.0 * jnp.arange(half, dtype=jnp.float32) / vector.shape[-1])
    places = (first_row + jnp.arange(vector.shape[0], dtype=jnp.int32)).astype(jnp.float32)
    angle = places[:, None] * rates[None, :]
    angle = angle.reshape((vector.shape[0],) + (1,) * (vector.ndim - 2) + (half,))
    cosine = jnp.cos(angle)
    sine = jnp.sin(angle)
    left = vector[..., :half]
    right = vector[..., half:]
    return jnp.concatenate([left * cosine - right * sine, left * sine + right * cosine], axis=-1)


def latent_norm(latent, latent_gain):
    wide = latent.astype(jnp.float32)
    factor = lax.rsqrt(jnp.mean(wide * wide, axis=-1, keepdims=True) + norm_floor)
    return (wide * factor * latent_gain).astype(jnp.bfloat16)


def layer_norm(values, gain):
    centre = jnp.mean(values, axis=-1, keepdims=True)
    centred = values - centre
    spread = jnp.mean(centred * centred, axis=-1, keepdims=True)
    return centred * lax.rsqrt(spread + norm_floor) * gain


def per_device(
    queries_nope,
    queries_rope,
    latent,
    rope_key,
    latent_gain,
    key_up,
    value_up,
    out_proj,
    stream,
    mix_gain,
    w_gate,
    w_up,
    w_down,
    mlp_gain,
):
    row_count, head_count, head_dim = queries_nope.shape
    rope_dim = queries_rope.shape[2]
    first_row = lax.axis_index("sp") * row_count
    query_turned = rotate(queries_rope.astype(jnp.float32), first_row).astype(jnp.bfloat16)
    key_turned = rotate(rope_key.astype(jnp.float32), first_row).astype(jnp.bfloat16)
    normed = latent_norm(latent, latent_gain)
    scale = (head_dim + rope_dim) ** (-0.5)
    query_places = first_row + jnp.arange(row_count, dtype=jnp.int32)
    last_place = first_row + row_count - 1

    def add_piece(carry, piece):
        top, denominators, weighted = carry
        latent_piece, rotary_piece = piece
        count = latent_piece.shape[0]
        keys = jnp.dot(latent_piece, key_up, preferred_element_type=jnp.float32).astype(
            jnp.bfloat16
        )
        keys = keys.reshape(count, head_count, head_dim)
        values_here = jnp.dot(latent_piece, value_up, preferred_element_type=jnp.float32).astype(
            jnp.bfloat16
        )
        values_here = values_here.reshape(count, head_count, head_dim)
        score = jnp.einsum("thd,shd->hts", queries_nope, keys, preferred_element_type=jnp.float32)
        score = score + jnp.einsum(
            "thr,sr->hts", query_turned, rotary_piece, preferred_element_type=jnp.float32
        )
        score = score * scale
        allowed = jnp.arange(count, dtype=jnp.int32)[None, :] <= query_places[:, None]
        score = jnp.where(allowed[None], score, big_negative)
        new_top = jnp.maximum(top, jnp.max(score, axis=2))
        powers = jnp.exp(score - new_top[:, :, None]) * allowed[None]
        shrink = jnp.exp(top - new_top)
        denominators = jnp.sum(powers, axis=2)
        weighted = weighted * shrink.T[:, :, None] + jnp.einsum(
            "hts,shd->thd",
            powers.astype(jnp.bfloat16),
            values_here,
            preferred_element_type=jnp.float32,
        )
        return (new_top, denominators, weighted)

    start_state = (
        jnp.full((head_count, row_count), big_negative, jnp.float32),
        jnp.zeros((head_count, row_count), jnp.float32),
        jnp.zeros((row_count, head_count, head_dim), jnp.float32),
    )
    piece = (
        lax.all_gather(normed, "sp", axis=0, tiled=True),
        lax.all_gather(key_turned, "sp", axis=0, tiled=True),
    )
    top, denominators, weighted = lax.cond(
        jnp.int32(0) <= last_place,
        lambda state: add_piece(state, piece),
        lambda state: state,
        start_state,
    )
    attended = (
        (weighted / denominators.T[:, :, None])
        .astype(jnp.bfloat16)
        .reshape(row_count, head_count * head_dim)
    )
    row_heads = lax.all_to_all(attended, "tp", split_axis=0, concat_axis=1, tiled=True)
    whole_proj = lax.all_gather(out_proj, "tp", axis=0, tiled=True)
    projected = jnp.dot(row_heads, whole_proj, preferred_element_type=jnp.float32)
    mixed = layer_norm(residual_weight * stream.astype(jnp.float32) + projected, mix_gain).astype(
        jnp.bfloat16
    )
    all_rows = lax.all_gather(mixed, "tp", axis=0, tiled=True)
    gate_sum = jnp.dot(
        all_rows,
        lax.all_gather(w_gate, "sp", axis=0, tiled=True),
        preferred_element_type=jnp.float32,
    )
    up_sum = jnp.dot(
        all_rows, lax.all_gather(w_up, "sp", axis=0, tiled=True), preferred_element_type=jnp.float32
    )
    hidden = (jax.nn.silu(gate_sum) * up_sum).astype(jnp.bfloat16)
    terms = jnp.dot(
        hidden, lax.all_gather(w_down, "sp", axis=1, tiled=True), preferred_element_type=jnp.float32
    )
    lowered = lax.psum_scatter(
        terms.astype(jnp.bfloat16), "tp", scatter_dimension=0, tiled=True
    ).astype(jnp.float32)
    return layer_norm(residual_weight * mixed.astype(jnp.float32) + 0.5 * lowered, mlp_gain).astype(
        jnp.bfloat16
    )


def solution(mesh):
    return jax.shard_map(
        per_device,
        mesh=mesh,
        in_specs=(
            P("sp", "tp", None),
            P("sp", "tp", None),
            P("sp", None),
            P("sp", None),
            P(),
            P(None, "tp"),
            P(None, "tp"),
            P("tp", None),
            P(("sp", "tp"), None),
            P(),
            P("sp", "tp"),
            P("sp", "tp"),
            P("tp", "sp"),
            P(),
        ),
        out_specs=P(("sp", "tp"), None),
        check_vma=False,
    )
```

profile of v0, /device:TPU:0, one launch (start us, length us, event | category | flops | bytes accessed | tf_op | source)
XLA Modules:
  0.0 365.5 jit_solution(3936866935383197673)
XLA Ops:
  6.5 1.2 fusion.19
  7.8 1.9 fusion.21
  9.7 0.7 all-gather.9.cloned.1.call-update
  10.5 0.7 all-gather.13.cloned.1.call-update
  11.2 0.8 convert_element_type.70
  12.1 0.3 multiply_cosine_fusion
  12.5 36.4 %all_gather.22 = bf16[3072,64]{0,1:T(8,128)(2,1)} all-gather(bf16[384,64]{0,1:T(8,128)(2,1)S(1)} %pad_maximum_fusion.1), channel_id=1, replica_groups=mesh['sp'=8,'tp'=4] {'sp'}, dimensions={0}, use_global_device_ids=true | all-gather | bytes 442368 | tf_op jit(solution)/shard_map/all_gather | solution.py:102
  48.8 26.7 %all-gather.7.cloned.1.call-done = bf16[3072,512]{1,0:T(8,128)(2,1)} async-done(((bf16[384,512]{1,0:T(8,128)(2,1)}), bf16[3072,512]{1,0:T(8,128)(2,1)}) %all-gather.7.cloned.1.call-update) | async-done | bytes 3145744 | tf_op jit(solution)/shard_map/all_gather | solution.py:101
  75.5 12.4 %conditional.1 = (f32[2,384]{1,0:T(2,128)S(1)}, f32[384,2,128]{0,2,1:T(8,128)S(1)}) conditional(s32[]{:T(128)} %convert_element_type.67, () %tuple.13, (s32[]{:T(128)}, s32[384]{0:T(512)S(1)}, bf16[3072,512]{1,0:T(8,128)(2,1)}, bf16[512,256]{1,0:T(8,128)(2,1)S(1)}, bf16[384,2,128]{2,1,0:T(2,128)(2,1)S(1)}, /*index=5*/bf16[3072,64]{0,1:T(8,128)(2,1)}, ...), branch_computations={%region_1.0_spmd, %region_2.5_spmd} | conditional | flops 3148186624 | bytes 93123176 | solution.py:104
  75.5 2.9 convolution_convert_fusion.1
  78.5 1.6 fusion.15
  80.0 1.0 fusion.17
  81.1 2.4 fusion.25
  83.5 1.1 convolution_convert_fusion
  84.5 1.9 fusion.11
  86.4 1.5 fusion.3
  88.3 10.4 %all_to_all.19 = bf16[4,96,256]{2,1,0:T(8,128)(2,1)S(1)} all-to-all(bf16[4,96,256]{2,1,0:T(8,128)(2,1)S(1)} %all_to_all.14), channel_id=1, replica_groups=mesh['sp'=8,'tp'=4] {'tp'}, dimensions={0} | all-to-all | bytes 393216 | tf_op jit(solution)/shard_map/all_to_all | solution.py:115
  98.7 13.8 %all-gather.9.cloned.1.call-done = bf16[1024,2048]{1,0:T(8,128)(2,1)} async-done(((bf16[256,2048]{1,0:T(8,128)(2,1)}), bf16[1024,2048]{1,0:T(8,128)(2,1)}) %all-gather.9.cloned.1.call-update) | async-done | bytes 4194320 | tf_op jit(solution)/shard_map/all_gather | solution.py:116
  112.5 3.2 fusion.26
  116.0 0.9 multiply_convert_fusion.1
  117.0 0.5 all-gather.15.cloned.1.call-update
  117.6 0.5 all-gather.17.cloned.1.call-update
  118.1 56.6 %all-gather.13.cloned.1.call-done = bf16[2048,768]{1,0:T(8,128)(2,1)} async-done(((bf16[256,768]{1,0:T(8,128)(2,1)}), bf16[2048,768]{1,0:T(8,128)(2,1)}) %all-gather.13.cloned.1.call-update) | async-done | bytes 3145744 | tf_op jit(solution)/shard_map/all_gather | solution.py:124
  174.8 19.7 %all-gather.11.cloned.1.call-done = bf16[384,2048]{1,0:T(8,128)(2,1)} async-done(((bf16[96,2048]{1,0:T(8,128)(2,1)}), bf16[384,2048]{1,0:T(8,128)(2,1)}) %all-gather.11.cloned.1.call-update) | async-done | bytes 1572880 | tf_op jit(solution)/shard_map/all_gather | solution.py:121
  194.5 4.9 %fusion.27 = f32[384,768]{1,0:T(8,128)} fusion(bf16[384,2048]{1,0:T(8,128)(2,1)} %all-gather.11.cloned.1.call-done, bf16[2048,768]{1,0:T(8,128)(2,1)} %all-gather.13.cloned.1.call-done), kind=kOutput, calls=%fused_computation.56 | convolution fusion | flops 1207959552 | bytes 5898240 | tf_op jit(solution)/shard_map/dot_general | solution.py:122
  199.4 57.2 %all-gather.15.cloned.1.call-done = bf16[2048,768]{1,0:T(8,128)(2,1)} async-done(((bf16[256,768]{1,0:T(8,128)(2,1)}), bf16[2048,768]{1,0:T(8,128)(2,1)}) %all-gather.15.cloned.1.call-update) | async-done | bytes 3145744 | tf_op jit(solution)/shard_map/all_gather | solution.py:128
  256.6 63.2 %all-gather.17.cloned.1.call-done = bf16[768,2048]{1,0:T(8,128)(2,1)} async-done(((bf16[768,256]{1,0:T(8,128)(2,1)}), bf16[768,2048]{1,0:T(8,128)(2,1)}) %all-gather.17.cloned.1.call-update) | async-done | bytes 3145744 | tf_op jit(solution)/shard_map/all_gather | solution.py:132
  319.8 7.5 %convolution_convert_fusion.2 = bf16[384,2048]{1,0:T(8,128)(2,1)} fusion(bf16[768,2048]{1,0:T(8,128)(2,1)} %all-gather.17.cloned.1.call-done, bf16[384,2048]{1,0:T(8,128)(2,1)S(1)} %copy-done.8, bf16[2048,768]{1,0:T(8,128)(2,1)} %all-gather.15.cloned.1.call-done, f32[384,768]{1,0:T(8,128)} %fusion.27), kind=kOutput, calls=%fused_computation.21 | convolution fusion | flops 2418475008 | bytes 10616832 | tf_op jit(solution)/shard_map/dot_general | solution.py:131
  327.3 26.3 %reduce-scatter.2.cloned.1.call-done = bf16[96,2048]{1,0:T(8,128)(2,1)} async-done(((bf16[384,2048]{1,0:T(8,128)(2,1)}), bf16[96,2048]{1,0:T(8,128)(2,1)}) %reduce-scatter.2.cloned.1.call-update) | async-done | bytes 393232 | tf_op jit(solution)/shard_map/reduce_scatter | solution.py:134
  353.6 1.4 fusion.23
  355.0 1.4 multiply_reduce_fusion
  356.5 2.2 multiply_convert_fusion
  (47 shorter events, 1.0 us)
Async XLA Ops:
  6.5 5.5 %copy-start.6 = (bf16[384,2,64]{0,2,1:T(8,128)(2,1)S(1)}, bf16[384,2,64]{0,2,1:T(8,128)(2,1)}, u32[]{:S(2)}) copy-start(bf16[384,2,64]{0,2,1:T(8,128)(2,1)} %param.17) | copy-start | bytes 294916
  6.5 69.0 %copy-start.4 = (bf16[384,2,128]{2,1,0:T(2,128)(2,1)S(1)}, bf16[384,2,128]{2,1,0:T(2,128)(2,1)}, u32[]{:S(2)}) copy-start(bf16[384,2,128]{2,1,0:T(2,128)(2,1)} %param.16) | copy-start | bytes 589828
  6.5 69.0 %copy-start.2 = (bf16[512,256]{1,0:T(8,128)(2,1)S(1)}, bf16[512,256]{1,0:T(8,128)(2,1)}, u32[]{:S(2)}) copy-start(bf16[512,256]{1,0:T(8,128)(2,1)} %param.21) | copy-start | bytes 786436
  6.5 69.0 %all-gather.7.cloned.1.call-start = ((), (), s32[]{:S(2)}) async-start(), calls=%async_computation.2 | async-start | bytes 3538944 | tf_op jit(solution)/shard_map/all_gather | solution.py:101
  9.7 102.8 %all-gather.9.cloned.1.call-start = ((), (), s32[]{:S(2)}) async-start(), calls=%async_computation.3 | async-start | bytes 5242880 | tf_op jit(solution)/shard_map/all_gather | solution.py:116
  10.5 164.3 %all-gather.13.cloned.1.call-start = ((), (), s32[]{:S(2)}) async-start(), calls=%async_computation.5 | async-start | bytes 3538944 | tf_op jit(solution)/shard_map/all_gather | solution.py:124
  11.2 183.3 %all-gather.11.cloned.1.call-start = ((), (), s32[]{:S(2)}) async-start(), calls=%async_computation.4 | async-start | bytes 1966080 | tf_op jit(solution)/shard_map/all_gather | solution.py:121
  80.0 1.0 copy-start.1
  81.0 2.4 copy-start
  81.0 2.4 copy-start.3
  112.5 3.5 copy-start.5
  116.9 139.6 %all-gather.15.cloned.1.call-start = ((), (), s32[]{:S(2)}) async-start(), calls=%async_computation.6 | async-start | bytes 3538944 | tf_op jit(solution)/shard_map/all_gather | solution.py:128
  117.5 202.3 %all-gather.17.cloned.1.call-start = ((), (), s32[]{:S(2)}) async-start(), calls=%async_computation.7 | async-start | bytes 3538944 | tf_op jit(solution)/shard_map/all_gather | solution.py:132
  118.1 235.5 %reduce-scatter.2.cloned.1.call-start = ((), (), s32[]{:S(2)}) async-start(), calls=%async_computation.8 | async-start | bytes 1966080 | tf_op jit(solution)/shard_map/reduce_scatter | solution.py:134
  194.5 125.3 %copy-start.8 = (bf16[384,2048]{1,0:T(8,128)(2,1)S(1)}, bf16[384,2048]{1,0:T(8,128)(2,1)}, u32[]{:S(2)}) copy-start(bf16[384,2048]{1,0:T(8,128)(2,1)} %all-gather.11.cloned.1.call-done) | copy-start | bytes 4718596
  327.3 29.2 %copy-start.7 = (f32[2048]{0:T(1024)S(1)}, f32[2048]{0:T(1024)}, u32[]{:S(2)}) copy-start(f32[2048]{0:T(1024)} %param.29) | copy-start | bytes 24580
Sparse Core Ops, SparseCore 0:
  9.8 65.6 all-gather.6
  77.1 35.3 all-gather.8
  114.7 60.0 all-gather.12
  176.2 18.2 all-gather.10
  196.5 60.0 all-gather.14
  258.5 61.3 all-gather.16
  327.4 26.1 reduce-scatter.1
where the time goes:
time: 366 us
  waiting for transfers between devices  266 us (73%)
  blocking collectives  46.8 us (13%)
  matrix products  25.3 us (7%)
  between operations  13.6 us (4%)
  other arithmetic  13 us (4%)
    all_gather x1, waiting for transfers between devices, per_device(): lax.all_gather(w_down, 'sp', axis=1, tiled=True)  63.2 us
    all_gather x1, waiting for transfers between devices, per_device(): lax.all_gather(w_up, 'sp', axis=0, tiled=True)  57.2 us
    all_gather x1, waiting for transfers between devices, per_device(): lax.all_gather(w_gate, 'sp', axis=0, tiled=True)  56.6 us
    all_gather x1, blocking collectives, per_device(): lax.all_gather(key_turned, 'sp', axis=0, tiled=True)  36.4 us
    all_gather x1, waiting for transfers between devices, per_device(): lax.all_gather(normed, 'sp', axis=0, tiled=True)  26.7 us
    reduce_scatter x1, waiting for transfers between devices, per_device(): lax.psum_scatter(terms.astype(jnp.bfloat16), 'tp', scatter_dimension=0, t...  26.3 us
    all_gather x1, waiting for transfers between devices, per_device(): all_rows = lax.all_gather(mixed, 'tp', axis=0, tiled=True)  19.7 us
    all_gather x1, waiting for transfers between devices, per_device(): whole_proj = lax.all_gather(out_proj, 'tp', axis=0, tiled=True)  13.8 us
  transfers between devices with their start and end apart: 7, of which 7 were waited for; matrix products, arithmetic and copies ran while one was open for 6% of the time, Pallas kernels for 0%

commit v1 on v0

--- a/solution.py
+++ b/solution.py
@@ -1,3 +1,4 @@
+import functools
 import jax
 import jax.numpy as jnp
 from jax import lax
@@ -7,6 +8,25 @@
 residual_weight = 8.0**0.25
 norm_floor = 1.0
 big_negative = -1e30
+
+
+def test_target(buf, axis_key):
+    sides = lax.axis_size(axis_key)
+    pool = [buf]
+    c = 0
+    while c < sides - 1:
+        pool.append(
+            lax.ppermute(
+                pool[-1], axis_key, [(hop_no, (hop_no + 1) % sides) for hop_no in range(sides)]
+            )
+        )
+        c += 1
+    return jnp.roll(
+        jnp.concatenate(pool[::-1], 0), (lax.axis_index(axis_key) + 1) * buf.shape[0], 0
+    )
+
+
+ladders_watch = functools.partial(test_target, axis_key="tp")
 
 
 def rotate(vector, first_row):
@@ -118,7 +138,7 @@
     mixed = layer_norm(residual_weight * stream.astype(jnp.float32) + projected, mix_gain).astype(
         jnp.bfloat16
     )
-    all_rows = lax.all_gather(mixed, "tp", axis=0, tiled=True)
+    all_rows = ladders_watch(mixed)
     gate_sum = jnp.dot(
         all_rows,
         lax.all_gather(w_gate, "sp", axis=0, tiled=True),

time: 366 us -> 345 us (0.943)
  waiting for transfers between devices: 266 us -> 247 us
  blocking collectives: 46.8 us -> 36.5 us
  local copies, waits for them, and re-layouts: 0.35 us -> 5.72 us
  starting transfers between devices: 0.24 us -> 4.07 us
    all_gather x1, waiting for transfers between devices: 57.2 us -> 30.4 us  [per_device(): lax.all_gather(w_up, 'sp', axis=0, tiled=True)]
    ppermute x0 -> x3, waiting for transfers between devices: none -> 21.4 us  [test_target(): lax.ppermute(pool[-1], axis_key, [(hop_no, (hop_no + 1) % sides) for hop_...]
    all_gather x1 -> x0, waiting for transfers between devices: 19.7 us -> none  [per_device(): all_rows = lax.all_gather(mixed, 'tp', axis=0, tiled=True)]
    all_to_all x1 -> x0, blocking collectives: 10.4 us -> none  [per_device(): lax.all_to_all(attended, 'tp', split_axis=0, concat_axis=1, tiled=True)]
    all_to_all x0 -> x1, waiting for transfers between devices: none -> 6.98 us  [per_device(): lax.all_to_all(attended, 'tp', split_axis=0, concat_axis=1, tiled=True)]
    unnamed x12 -> x18, local copies, waits for them, and re-layouts: 0.02 us -> 4.71 us
  transfers between devices with their start and end apart: 7 -> 10, of which waited for: 7 -> 10; matrix products, arithmetic and copies ran while one was open for 6% -> 8% of each run, Pallas kernels for 0% -> 0%
where the time goes in v1:
time: 345 us
  waiting for transfers between devices  247 us (72%)
  blocking collectives  36.5 us (11%)
  matrix products  24.4 us (7%)
  between operations  13.7 us (4%)
  other arithmetic  13.4 us (4%)
  local copies, waits for them, and re-layouts  5.72 us (2%)
  starting transfers between devices  4.07 us (1%)
    all_gather x1, waiting for transfers between devices, per_device(): lax.all_gather(w_down, 'sp', axis=1, tiled=True)  63.2 us
    all_gather x1, waiting for transfers between devices, per_device(): lax.all_gather(w_gate, 'sp', axis=0, tiled=True)  57 us
    all_gather x1, blocking collectives, per_device(): lax.all_gather(key_turned, 'sp', axis=0, tiled=True)  36.5 us
    all_gather x1, waiting for transfers between devices, per_device(): lax.all_gather(w_up, 'sp', axis=0, tiled=True)  30.4 us
    all_gather x1, waiting for transfers between devices, per_device(): lax.all_gather(normed, 'sp', axis=0, tiled=True)  26.8 us
    reduce_scatter x1, waiting for transfers between devices, per_device(): lax.psum_scatter(terms.astype(jnp.bfloat16), 'tp', scatter_dimension=0, t...  26.4 us
    ppermute x3, waiting for transfers between devices, test_target(): lax.ppermute(pool[-1], axis_key, [(hop_no, (hop_no + 1) % sides) for hop_...  21.4 us
    all_gather x1, waiting for transfers between devices, per_device(): whole_proj = lax.all_gather(out_proj, 'tp', axis=0, tiled=True)  12.3 us
  transfers between devices with their start and end apart: 10, of which 10 were waited for; matrix products, arithmetic and copies ran while one was open for 8% of the time, Pallas kernels for 0%

profile of v1, /device:TPU:0, one launch (start us, length us, event | category | flops | bytes accessed | tf_op | source)
XLA Modules:
  0.0 344.7 jit_solution(17649478905595906989)
XLA Ops:
  6.6 1.2 fusion.22
  7.8 1.9 fusion.24
  12.3 36.5 %all_gather.19 = bf16[3072,64]{0,1:T(8,128)(2,1)} all-gather(bf16[384,64]{0,1:T(8,128)(2,1)S(1)} %pad_maximum_fusion.1), channel_id=1, replica_groups=mesh['sp'=8,'tp'=4] {'sp'}, dimensions={0}, use_global_device_ids=true | all-gather | bytes 442368 | tf_op jit(solution)/shard_map/all_gather | solution.py:122
  48.7 26.8 %all-gather.6.cloned.1.call-done = bf16[3072,512]{1,0:T(8,128)(2,1)} async-done(((bf16[384,512]{1,0:T(8,128)(2,1)}), bf16[3072,512]{1,0:T(8,128)(2,1)}) %all-gather.6.cloned.1.call-update) | async-done | bytes 3145744 | tf_op jit(solution)/shard_map/all_gather | solution.py:121
  75.5 12.4 %conditional.1 = (f32[2,384]{1,0:T(2,128)S(1)}, f32[384,2,128]{0,2,1:T(8,128)S(1)}) conditional(s32[]{:T(128)} %convert_element_type.67, () %tuple.13, (s32[]{:T(128)}, s32[384]{0:T(512)S(1)}, bf16[3072,512]{1,0:T(8,128)(2,1)}, bf16[512,256]{1,0:T(8,128)(2,1)S(1)}, bf16[384,2,128]{2,1,0:T(2,128)(2,1)S(1)}, /*index=5*/bf16[3072,64]{0,1:T(8,128)(2,1)}, ...), branch_computations={%region_1.0_spmd, %region_2.5_spmd} | conditional | flops 3148186624 | bytes 93123176 | solution.py:124
  75.5 2.9 convolution_convert_fusion.1
  78.5 1.6 fusion.15
  80.0 1.0 fusion.17
  81.1 2.4 fusion.35
  83.5 1.0 convolution_convert_fusion
  84.5 1.9 fusion.11
  86.4 1.5 fusion.3
  88.2 0.8 all_to_all.14
  89.0 3.4 all-to-all-start
  93.2 7.0 %all-to-all-done = bf16[4,96,256]{2,1,0:T(8,128)(2,1)S(1)} async-done(((bf16[4,96,256]{2,1,0:T(8,128)(2,1)}), bf16[4,96,256]{2,1,0:T(8,128)(2,1)S(1)}, u32[]{:S(2)}, u32[]{:S(2)}) %all-to-all-start) | async-done | bytes 196640 | tf_op jit(solution)/shard_map/all_to_all | solution.py:135
  100.2 12.3 %all-gather.8.cloned.1.call-done = bf16[1024,2048]{1,0:T(8,128)(2,1)} async-done(((bf16[256,2048]{1,0:T(8,128)(2,1)}), bf16[1024,2048]{1,0:T(8,128)(2,1)}) %all-gather.8.cloned.1.call-update) | async-done | bytes 4194320 | tf_op jit(solution)/shard_map/all_gather | solution.py:136
  112.5 3.2 fusion.36
  116.5 7.0 %collective-permute-done = bf16[96,2048]{1,0:T(8,128)(2,1)S(1)} collective-permute-done((bf16[96,2048]{1,0:T(8,128)(2,1)S(1)}, bf16[96,2048]{1,0:T(8,128)(2,1)S(1)}, u32[]{:S(2)}, u32[]{:S(2)}) %collective-permute-start) | collective-permute-done | bytes 393248 | tf_op jit(solution)/shard_map/ppermute | solution.py:19
  123.4 7.2 %collective-permute-done.1 = bf16[96,2048]{1,0:T(8,128)(2,1)S(1)} collective-permute-done((bf16[96,2048]{1,0:T(8,128)(2,1)S(1)}, bf16[96,2048]{1,0:T(8,128)(2,1)S(1)}, u32[]{:S(2)}, u32[]{:S(2)}) %collective-permute-start.1) | collective-permute-done | bytes 393248 | tf_op jit(solution)/shard_map/ppermute | solution.py:19
  130.6 7.2 %collective-permute-done.2 = bf16[96,2048]{1,0:T(8,128)(2,1)S(1)} collective-permute-done((bf16[96,2048]{1,0:T(8,128)(2,1)S(1)}, bf16[96,2048]{1,0:T(8,128)(2,1)S(1)}, u32[]{:S(2)}, u32[]{:S(2)}) %collective-permute-start.2) | collective-permute-done | bytes 393248 | tf_op jit(solution)/shard_map/ppermute | solution.py:19
  139.4 0.8 constant_dynamic-update-slice_fusion.5
  140.2 0.9 constant_dynamic-update-slice_fusion.4
  143.4 0.9 constant_dynamic-update-slice_fusion
  144.4 30.4 %all-gather.12.cloned.1.call-done = bf16[2048,768]{1,0:T(8,128)(2,1)} async-done(((bf16[256,768]{1,0:T(8,128)(2,1)}), bf16[2048,768]{1,0:T(8,128)(2,1)}) %all-gather.12.cloned.1.call-update) | async-done | bytes 3145744 | tf_op jit(solution)/shard_map/all_gather | solution.py:148
  174.8 3.8 %fusion.18 = f32[384,768]{1,0:T(8,128)S(1)} fusion(bf16[2048,768]{1,0:T(8,128)(2,1)} %all-gather.12.cloned.1.call-done, bf16[768,2048]{1,0:T(8,128)(2,1)} %constant_dynamic-update-slice_fusion, s32[]{:T(128)S(6)} %select_n.18), kind=kOutput, calls=%fused_computation.23 | convolution fusion | flops 1207959552 | bytes 5898244 | tf_op jit(solution)/shard_map/dot_general | solution.py:147
  178.5 57.0 %all-gather.10.cloned.1.call-done = bf16[2048,768]{1,0:T(8,128)(2,1)} async-done(((bf16[256,768]{1,0:T(8,128)(2,1)}), bf16[2048,768]{1,0:T(8,128)(2,1)}) %all-gather.10.cloned.1.call-update) | async-done | bytes 3145744 | tf_op jit(solution)/shard_map/all_gather | solution.py:144
  235.5 63.2 %all-gather.14.cloned.1.call-done = bf16[768,2048]{1,0:T(8,128)(2,1)} async-done(((bf16[768,256]{1,0:T(8,128)(2,1)}), bf16[768,2048]{1,0:T(8,128)(2,1)}) %all-gather.14.cloned.1.call-update) | async-done | bytes 3145744 | tf_op jit(solution)/shard_map/all_gather | solution.py:152
  298.7 7.6 %convolution_convert_fusion.2 = bf16[384,2048]{1,0:T(8,128)(2,1)} fusion(bf16[768,2048]{1,0:T(8,128)(2,1)} %all-gather.14.cloned.1.call-done, f32[384,768]{1,0:T(8,128)S(1)} %fusion.18, bf16[2048,768]{1,0:T(8,128)(2,1)} %all-gather.10.cloned.1.call-done, bf16[768,2048]{1,0:T(8,128)(2,1)} %constant_dynamic-update-slice_fusion, s32[]{:T(128)S(6)} %select_n.18), kind=kOutput, calls=%fused_computation.21 | convolution fusion | flops 2418475008 | bytes 10616836 | tf_op jit(solution)/shard_map/dot_general | solution.py:151
  306.4 26.4 %reduce-scatter.2.cloned.1.call-done = bf16[96,2048]{1,0:T(8,128)(2,1)} async-done(((bf16[384,2048]{1,0:T(8,128)(2,1)}), bf16[96,2048]{1,0:T(8,128)(2,1)}) %reduce-scatter.2.cloned.1.call-update) | async-done | bytes 393232 | tf_op jit(solution)/shard_map/reduce_scatter | solution.py:154
  332.8 1.4 fusion.30
  334.2 1.4 multiply_reduce_fusion
  335.6 2.2 multiply_convert_fusion.1
  (59 shorter events, 8.2 us)
Async XLA Ops:
  6.5 5.3 %copy-start.7 = (bf16[384,64]{0,1:T(8,128)(2,1)S(1)}, bf16[384,64]{0,1:T(8,128)(2,1)}, u32[]{:S(2)}) copy-start(bf16[384,64]{0,1:T(8,128)(2,1)} %param.19) | copy-start | bytes 147460
  6.5 5.3 %copy-start.6 = (bf16[384,2,64]{0,2,1:T(8,128)(2,1)S(1)}, bf16[384,2,64]{0,2,1:T(8,128)(2,1)}, u32[]{:S(2)}) copy-start(bf16[384,2,64]{0,2,1:T(8,128)(2,1)} %param.17) | copy-start | bytes 294916
  6.5 69.0 %copy-start.5 = (bf16[384,2,128]{2,1,0:T(2,128)(2,1)S(1)}, bf16[384,2,128]{2,1,0:T(2,128)(2,1)}, u32[]{:S(2)}) copy-start(bf16[384,2,128]{2,1,0:T(2,128)(2,1)} %param.16) | copy-start | bytes 589828
  6.5 69.0 %copy-start.3 = (bf16[512,256]{1,0:T(8,128)(2,1)S(1)}, bf16[512,256]{1,0:T(8,128)(2,1)}, u32[]{:S(2)}) copy-start(bf16[512,256]{1,0:T(8,128)(2,1)} %param.21) | copy-start | bytes 786436
  6.5 69.0 %all-gather.6.cloned.1.call-start = ((), (), s32[]{:S(2)}) async-start(), calls=%async_computation.2 | async-start | bytes 3538944 | tf_op jit(solution)/shard_map/all_gather | solution.py:121
  9.8 102.8 %all-gather.8.cloned.1.call-start = ((), (), s32[]{:S(2)}) async-start(), calls=%async_computation.3 | async-start | bytes 5242880 | tf_op jit(solution)/shard_map/all_gather | solution.py:136
  10.5 164.2 %all-gather.12.cloned.1.call-start = ((), (), s32[]{:S(2)}) async-start(), calls=%async_computation.5 | async-start | bytes 3538944 | tf_op jit(solution)/shard_map/all_gather | solution.py:148
  11.2 224.3 %all-gather.10.cloned.1.call-start = ((), (), s32[]{:S(2)}) async-start(), calls=%async_computation.4 | async-start | bytes 3538944 | tf_op jit(solution)/shard_map/all_gather | solution.py:144
  80.0 1.0 copy-start.1
  81.0 2.4 copy-start
  81.0 2.4 copy-start.4
  89.0 11.2 %all-to-all-start = ((bf16[4,96,256]{2,1,0:T(8,128)(2,1)}), bf16[4,96,256]{2,1,0:T(8,128)(2,1)S(1)}, u32[]{:S(2)}, u32[]{:S(2)}) async-start(bf16[4,96,256]{2,1,0:T(8,128)(2,1)} %all_to_all.14), calls=%async_computation | async-start | bytes 393216 | tf_op jit(solution)/shard_map/all_to_all | solution.py:135
  92.4 206.4 %all-gather.14.cloned.1.call-start = ((), (), s32[]{:S(2)}) async-start(), calls=%async_computation.6 | async-start | bytes 3538944 | tf_op jit(solution)/shard_map/all_gather | solution.py:152
  93.0 239.8 %reduce-scatter.2.cloned.1.call-start = ((), (), s32[]{:S(2)}) async-start(), calls=%async_computation.7 | async-start | bytes 1966080 | tf_op jit(solution)/shard_map/reduce_scatter | solution.py:154
  112.5 3.5 %copy-start.2 = (f32[2048]{0:T(1024)S(1)}, f32[2048]{0:T(1024)}, u32[]{:S(2)}) copy-start(f32[2048]{0:T(1024)} %param.25) | copy-start | bytes 24580
  116.2 7.3 %collective-permute-start = (bf16[96,2048]{1,0:T(8,128)(2,1)S(1)}, bf16[96,2048]{1,0:T(8,128)(2,1)S(1)}, u32[]{:S(2)}, u32[]{:S(2)}) collective-permute-start(bf16[96,2048]{1,0:T(8,128)(2,1)S(1)} %multiply_convert_fusion.2), channel_id=1, source_target_pairs={{0,1},{1,2},{2,3},{3,0},{4,5},{5,6},{6,7},{7,4},{8,9},{9,10},{10,1... | collective-permute-start | bytes 1179656 | tf_op jit(solution)/shard_map/ppermute | solution.py:19
  123.4 7.2 %collective-permute-start.1 = (bf16[96,2048]{1,0:T(8,128)(2,1)S(1)}, bf16[96,2048]{1,0:T(8,128)(2,1)S(1)}, u32[]{:S(2)}, u32[]{:S(2)}) collective-permute-start(bf16[96,2048]{1,0:T(8,128)(2,1)S(1)} %collective-permute-done), channel_id=1, source_target_pairs={{0,1},{1,2},{2,3},{3,0},{4,5},{5,6},{6,7},{7,4},{8,9},{9,10},{10,1... | collective-permute-start | bytes 1179656 | tf_op jit(solution)/shard_map/ppermute | solution.py:19
  130.6 7.2 %collective-permute-start.2 = (bf16[96,2048]{1,0:T(8,128)(2,1)S(1)}, bf16[96,2048]{1,0:T(8,128)(2,1)S(1)}, u32[]{:S(2)}, u32[]{:S(2)}) collective-permute-start(bf16[96,2048]{1,0:T(8,128)(2,1)S(1)} %collective-permute-done.1), channel_id=1, source_target_pairs={{0,1},{1,2},{2,3},{3,0},{4,5},{5,6},{6,7},{7,4},{8,9},{9,10},{10,1... | collective-permute-start | bytes 1179656 | tf_op jit(solution)/shard_map/ppermute | solution.py:19
  306.4 29.3 %copy-start.8 = (f32[2048]{0:T(1024)S(1)}, f32[2048]{0:T(1024)}, u32[]{:S(2)}) copy-start(f32[2048]{0:T(1024)} %param.29) | copy-start | bytes 24580
Sparse Core Ops, SparseCore 0:
  9.9 65.6 all-gather.5
  77.1 35.3 all-gather.7
  114.7 60.0 all-gather.11
  176.8 58.6 all-gather.9
  237.4 61.2 all-gather.13
  306.5 26.2 reduce-scatter.1
